TPU v7x, 32 devices: a whole 2x2x4 slice. The times are simulated.
32 devices in a mesh: ep: 4 (over z), tp: 8 (over y, x, core).
Axes of the slice: x: 2, y: 2, z: 4, core: 2. Of those that a mesh axis runs over, the one named last changes fastest.
Arguments:
- tokens: bfloat16 [512, 2048], P('ep', 'tp'), may hold values from -6 to 6
- out_grad: bfloat16 [512, 2048], P('ep', 'tp'), may hold values from -6 to 6
- routes: int32 [512, 2], P('ep'), may hold values from 0 to 3, all different within a row; in each aligned block of 128 rows (0 to 127, 128 to 255, ...) at most 96 rows name the same one
- gates: float32 [512, 2], P('ep'), may hold values from 0.1 to 0.9
- gate_weight: bfloat16 [4, 2048, 5632], P('ep', None, 'tp'), may hold values from -0.125 to 0.125
- up_weight: bfloat16 [4, 2048, 5632], P('ep', None, 'tp'), may hold values from -0.125 to 0.125
- down_weight: bfloat16 [4, 5632, 2048], P('ep', 'tp'), may hold values from -0.078125 to 0.078125
Outputs:
- tokens_grad: bfloat16 [512, 2048], P('ep', 'tp')
- gates_grad: float32 [512, 2], P(('ep', 'tp'))
- gate_weight_grad: bfloat16 [4, 2048, 5632], P('ep', None, 'tp')
- up_weight_grad: bfloat16 [4, 2048, 5632], P('ep', None, 'tp')
- down_weight_grad: bfloat16 [4, 5632, 2048], P('ep', 'tp')
Inputs may be any that keep to these rules, and one draw needn't show every extreme that they name: `routes`: the 2 experts of a token differ. In each aligned block of 128 rows (the tokens of one index of ep) no expert is named by more than 96 rows, a bound that some block reaches.
All inputs are finite; a program needn't handle non-finite values.
Results may differ from a plain program's by a relative error of at most 0.029.
Values may be sent and summed in bfloat16 or wider, within the bound.
A program may use at most 64 MiB of HBM per device.

v0:
```python
import jax
import jax.numpy as jnp
from jax import lax
from jax.sharding import PartitionSpec as P


def expert_grads(rows, cotan, w_gate, w_up, w_down):
    pre_gate = jnp.dot(rows, w_gate, preferred_element_type=jnp.float32)
    pre_up = jnp.dot(rows, w_up, preferred_element_type=jnp.float32)
    activated = jax.nn.silu(pre_gate)
    hidden = (activated * pre_up).astype(jnp.bfloat16)
    hid_grad = jnp.dot(cotan, w_down.T, preferred_element_type=jnp.float32)
    sigmoid_gate = jax.nn.sigmoid(pre_gate)
    gate_part = (hid_grad * pre_up * sigmoid_gate * (1.0 + pre_gate * (1.0 - sigmoid_gate))).astype(
        jnp.bfloat16
    )
    up_part = (hid_grad * activated).astype(jnp.bfloat16)
    slot_dots = jnp.sum(hidden.astype(jnp.float32) * hid_grad, axis=1)
    down_grad = jnp.dot(hidden.T, cotan, preferred_element_type=jnp.float32).astype(jnp.bfloat16)
    gate_grad = jnp.dot(rows.T, gate_part, preferred_element_type=jnp.float32).astype(jnp.bfloat16)
    up_grad = jnp.dot(rows.T, up_part, preferred_element_type=jnp.float32).astype(jnp.bfloat16)
    return (gate_part, up_part, slot_dots, gate_grad, up_grad, down_grad)


def on_device(tokens, out_grad, routes, gates, gate_weight, up_weight, down_weight):
    tok_dev, top_k = routes.shape
    ep_size = lax.axis_size("ep")
    tp_size = lax.axis_size("tp")
    capacity = (3 * tok_dev + ep_size - 1) // ep_size
    buffer_rows = ep_size * capacity
    slice_width = tokens.shape[1]
    flat_expert = routes.reshape(-1)
    onehot = (flat_expert[:, None] == jnp.arange(ep_size, dtype=jnp.int32)[None, :]).astype(
        jnp.int32
    )
    slot_rank = jnp.sum((jnp.cumsum(onehot, axis=0) - onehot) * onehot, axis=1)
    slot_dest = flat_expert * capacity + slot_rank
    placed = jnp.arange(buffer_rows, dtype=jnp.int32)[:, None] == slot_dest[None, :]
    placed_float = placed.astype(jnp.float32)
    select = jnp.any(placed.reshape(buffer_rows, tok_dev, top_k), axis=2).astype(jnp.bfloat16)
    slot_gate = jnp.dot(placed_float, gates.reshape(-1), precision=lax.Precision.HIGHEST)
    sent_rows = jnp.dot(select, tokens, preferred_element_type=jnp.float32).astype(jnp.bfloat16)
    cotan_rows = jnp.dot(select, out_grad, preferred_element_type=jnp.float32)
    sent_cotan = (slot_gate[:, None] * cotan_rows).astype(jnp.bfloat16)
    recv_rows, recv_cotan = (
        lax.all_to_all(
            sent_rows.reshape(ep_size, capacity, slice_width),
            "ep",
            split_axis=0,
            concat_axis=0,
            tiled=True,
        ),
        lax.all_to_all(
            sent_cotan.reshape(ep_size, capacity, slice_width),
            "ep",
            split_axis=0,
            concat_axis=0,
            tiled=True,
        ),
    )
    whole_rows, whole_cotan = (
        lax.all_gather(recv_rows, "tp", axis=2, tiled=True),
        lax.all_gather(recv_cotan, "tp", axis=2, tiled=True),
    )
    model_width = whole_rows.shape[2]
    rows = whole_rows.reshape(buffer_rows, model_width)
    cotan = whole_cotan.reshape(buffer_rows, model_width)
    w_gate = gate_weight[0]
    w_up = up_weight[0]
    gate_part, up_part, slot_dots, gate_grad, up_grad, down_grad = expert_grads(
        rows, cotan, w_gate, w_up, down_weight[0]
    )
    partial_value = jnp.dot(gate_part, w_gate.T, preferred_element_type=jnp.float32)
    partial_value = (
        partial_value + jnp.dot(up_part, w_up.T, preferred_element_type=jnp.float32)
    ).astype(jnp.bfloat16)
    share = tok_dev // tp_size
    start = lax.axis_index("tp") * share
    summed = lax.psum(slot_dots, "tp")
    row_sums = lax.psum_scatter(
        partial_value.reshape(ep_size, capacity, model_width), "tp", scatter_dimension=2, tiled=True
    ).astype(jnp.float32)
    back_rows, back_dots = (
        lax.all_to_all(
            row_sums.astype(jnp.bfloat16), "ep", split_axis=0, concat_axis=0, tiled=True
        ).astype(row_sums.dtype),
        lax.all_to_all(
            summed.reshape(ep_size, capacity).astype(jnp.bfloat16),
            "ep",
            split_axis=0,
            concat_axis=0,
            tiled=True,
        ).astype(jnp.float32),
    )
    slot_rows = back_rows.reshape(buffer_rows, slice_width)[slot_dest]
    tokens_grad = jnp.sum(slot_rows.reshape(tok_dev, top_k, slice_width), axis=1).astype(
        jnp.bfloat16
    )
    token_dots = back_dots.reshape(buffer_rows)[slot_dest].reshape(tok_dev, top_k)
    own_dots = lax.dynamic_slice_in_dim(token_dots, start, share, 0)
    own_gates = lax.dynamic_slice_in_dim(gates, start, share, 0)
    gates_grad = own_dots / own_gates
    return (tokens_grad, gates_grad, gate_grad[None], up_grad[None], down_grad[None])


def solution(mesh):
    placed = (
        P("ep", "tp"),
        P("ep", "tp"),
        P("ep", None),
        P("ep", None),
        P("ep", None, "tp"),
        P("ep", None, "tp"),
        P("ep", "tp", None),
    )
    return jax.shard_map(
        on_device,
        mesh=mesh,
        in_specs=placed,
        out_specs=(
            P("ep", "tp"),
            P(("ep", "tp"), None),
            P("ep", None, "tp"),
            P("ep", None, "tp"),
            P("ep", "tp", None),
        ),
        check_vma=False,
    )
```

profile of v0, /device:TPU:0, one launch (start us, length us, event | category | flops | bytes accessed | tf_op | source)
XLA Modules:
  0.0 148.4 jit_solution(13399779016683613916)
XLA Ops:
  7.2 0.9 copy.32
  8.5 1.2 reduce-window.6
  11.0 1.0 convolution_convert_fusion.3
  12.1 13.7 %all_to_all.21 = bf16[4,96,256]{2,1,0:T(8,128)(2,1)} all-to-all(bf16[4,96,256]{2,1,0:T(8,128)(2,1)S(1)} %bitcast.70), channel_id=1, replica_groups=mesh['ep'=4,'tp'=8] {'ep'}, dimensions={0} | all-to-all | bytes 393216 | tf_op jit(solution)/shard_map/all_to_all | solution.py:46
  26.7 9.9 %all_to_all.22 = bf16[4,96,256]{2,1,0:T(8,128)(2,1)} all-to-all(bf16[4,96,256]{2,1,0:T(8,128)(2,1)S(1)} %bitcast.69), channel_id=1, replica_groups=mesh['ep'=4,'tp'=8] {'ep'}, dimensions={0} | all-to-all | bytes 393216 | tf_op jit(solution)/shard_map/all_to_all | solution.py:53
  36.6 14.2 %all-gather.5.cloned.1.call-done = bf16[4,96,2048]{2,1,0:T(8,128)(2,1)} async-done(((bf16[4,96,256]{2,1,0:T(8,128)(2,1)}), bf16[4,96,2048]{2,1,0:T(8,128)(2,1)}) %all-gather.5.cloned.1.call-update) | async-done | bytes 1572880 | tf_op jit(solution)/shard_map/all_gather | solution.py:62
  50.9 4.2 %fusion.5 = f32[384,704]{0,1:T(8,128)} fusion(bf16[384,2048]{1,0:T(8,128)(2,1)} %bitcast.74, bf16[1,2048,704]{1,2,0:T(8,128)(2,1)S(1)} %copy-done), kind=kOutput, calls=%fused_computation.11 | convolution fusion | flops 1107296256 | bytes 5537792 | tf_op jit(solution)/shard_map/dot_general | solution.py:8
  55.1 2.7 %fusion.9 = f32[384,704]{0,1:T(8,128)} fusion(bf16[384,2048]{1,0:T(8,128)(2,1)S(1)} %bitcast.76, bf16[1,2048,704]{1,2,0:T(8,128)(2,1)S(1)} %copy-done.1), kind=kOutput, calls=%fused_computation.15 | convolution fusion | flops 1107296256 | bytes 5537792 | tf_op jit(solution)/shard_map/dot_general | solution.py:9
  57.8 20.8 %all-gather.3.cloned.1.call-done = bf16[4,96,2048]{2,1,0:T(8,128)(2,1)} async-done(((bf16[4,96,256]{2,1,0:T(8,128)(2,1)}), bf16[4,96,2048]{2,1,0:T(8,128)(2,1)}) %all-gather.3.cloned.1.call-update) | async-done | bytes 1572880 | tf_op jit(solution)/shard_map/all_gather | solution.py:63
  78.6 5.7 %multiply_reduce_fusion = (f32[384]{0:T(512)S(1)}, bf16[384,704]{0,1:T(8,128)(2,1)}, bf16[384,704]{0,1:T(8,128)(2,1)S(1)}, bf16[384,704]{0,1:T(8,128)(2,1)S(1)}) fusion(f32[384,704]{0,1:T(8,128)} %fusion.9, f32[384,704]{0,1:T(8,128)} %fusion.5, bf16[384,2048]{1,0:T(8,128)(2,1)} %bitcast.78, bf16[1,704,2048]{2,1,0:T(8,128)(2,1)} %param.13), kind=kOutput, calls=%fused_computation.23 | convolution fusion | flops 1112161920 | bytes 8242688 | tf_op jit(solution)/shard_map/dot_general | solution.py:12
  84.3 1.4 fusion.3
  86.3 2.6 %add_convert_fusion = bf16[384,2048]{1,0:T(8,128)(2,1)} fusion(f32[384,2048]{1,0:T(8,128)S(1)} %fusion.3, bf16[384,704]{0,1:T(8,128)(2,1)S(1)} %get-tuple-element.23, bf16[1,2048,704]{1,2,0:T(8,128)(2,1)S(1)} %copy-done.2), kind=kOutput, calls=%fused_computation.5 | convolution fusion | flops 1108869120 | bytes 8142848 | tf_op jit(solution)/shard_map/dot_general | solution.py:75
  89.0 1.0 mul.77
  90.0 13.1 %psum.7 = bf16[384]{0:T(512)(128)(2,1)S(1)} all-reduce(f32[384]{0:T(512)S(1)} %get-tuple-element.20), channel_id=1, replica_groups=mesh['ep'=4,'tp'=8] {'tp'}, use_global_device_ids=true, to_apply=%region_7.8 | all-reduce | flops 384 | bytes 2304 | tf_op jit(solution)/shard_map/psum | solution.py:79
  103.1 0.7 convert_element_type.83
  103.8 4.6 %all-to-all-start.3 = ((bf16[4,1,96]{2,1,0:T(2,128)(2,1)}), bf16[4,1,96]{2,1,0:T(2,128)(2,1)S(1)}, u32[]{:S(2)}, u32[]{:S(2)}) async-start(bf16[4,1,96]{2,1,0:T(2,128)(2,1)} %convert_element_type.83), calls=%async_computation.4 | async-start | bytes 4096 | tf_op jit(solution)/shard_map/all_to_all | solution.py:87
  108.4 5.0 %fusion.1 = bf16[1,2048,704]{1,2,0:T(8,128)(2,1)} fusion(bf16[384,704]{0,1:T(8,128)(2,1)S(1)} %get-tuple-element.22, bf16[384,2048]{1,0:T(8,128)(2,1)} %bitcast.75), kind=kOutput, calls=%fused_computation.7 | convolution fusion | flops 1108738048 | bytes 4997120 | tf_op jit(solution)/shard_map/dot_general | solution.py:20
  113.4 3.2 %fusion.2 = bf16[1,2048,704]{1,2,0:T(8,128)(2,1)} fusion(bf16[384,704]{0,1:T(8,128)(2,1)S(1)} %copy-done.4, bf16[384,2048]{1,0:T(8,128)(2,1)S(1)} %bitcast.77), kind=kOutput, calls=%fused_computation.8 | convolution fusion | flops 1108738048 | bytes 4997120 | tf_op jit(solution)/shard_map/dot_general | solution.py:21
  116.7 10.8 %reduce-scatter.2.cloned.1.call-done = bf16[4,96,256]{2,1,0:T(8,128)(2,1)} async-done(((bf16[4,96,2048]{2,1,0:T(8,128)(2,1)}), bf16[4,96,256]{2,1,0:T(8,128)(2,1)}) %reduce-scatter.2.cloned.1.call-update) | async-done | bytes 196624 | tf_op jit(solution)/shard_map/reduce_scatter | solution.py:80
  127.5 4.6 %all-to-all-start.2 = ((bf16[4,96,256]{2,1,0:T(8,128)(2,1)}), bf16[4,96,256]{2,1,0:T(8,128)(2,1)S(1)}, u32[]{:S(2)}, u32[]{:S(2)}) async-start(bf16[4,96,256]{2,1,0:T(8,128)(2,1)} %reduce-scatter.2.cloned.1.call-done), calls=%async_computation.3 | async-start | bytes 393216 | tf_op jit(solution)/shard_map/all_to_all | solution.py:84
  132.1 4.8 %fusion = bf16[1,704,2048]{2,1,0:T(8,128)(2,1)} fusion(bf16[384,704]{0,1:T(8,128)(2,1)} %get-tuple-element.21, bf16[384,2048]{1,0:T(8,128)(2,1)} %bitcast.79), kind=kOutput, calls=%fused_computation.6 | convolution fusion | flops 1108738048 | bytes 4997120 | tf_op jit(solution)/shard_map/dot_general | solution.py:19
  137.0 1.9 %gather_fusion.1 = f32[256]{0:T(256)S(1)} fusion(f32[384]{0:T(512)S(1)} %reshape.139, s32[1024]{0:T(1024)S(1)} %pad_clamp_fusion), kind=kCustom, calls=%fused_computation.1 | custom fusion | bytes 3072 | tf_op jit(solution)/shard_map/gather | solution.py:99
  139.8 1.0 gather_fusion
  140.9 0.9 reduce_sum.34
  (54 shorter events, 4.2 us)
Async XLA Ops:
  7.2 43.7 %copy-start = (bf16[1,2048,704]{1,2,0:T(8,128)(2,1)S(1)}, bf16[1,2048,704]{1,2,0:T(8,128)(2,1)}, u32[]{:S(2)}) copy-start(bf16[1,2048,704]{1,2,0:T(8,128)(2,1)} %param.11) | copy-start | bytes 8650756
  7.2 18.7 %copy-start.6 = (f32[128,2]{0,1:T(2,128)S(1)}, f32[128,2]{0,1:T(2,128)}, u32[]{:S(2)}) copy-start(f32[128,2]{0,1:T(2,128)} %param.10) | copy-start | bytes 3076
  7.2 19.3 %copy-start.5 = (bf16[128,256]{1,0:T(8,128)(2,1)S(1)}, bf16[128,256]{1,0:T(8,128)(2,1)}, u32[]{:S(2)}) copy-start(bf16[128,256]{1,0:T(8,128)(2,1)} %param.8) | copy-start | bytes 196612
  7.2 43.7 %all-gather.5.cloned.1.call-start = ((), (), s32[]{:S(2)}) async-start(), calls=%async_computation.6 | async-start | bytes 1769472 | tf_op jit(solution)/shard_map/all_gather | solution.py:62
  25.8 52.7 %all-gather.3.cloned.1.call-start = ((), (), s32[]{:S(2)}) async-start(), calls=%async_computation.5 | async-start | bytes 1769472 | tf_op jit(solution)/shard_map/all_gather | solution.py:63
  36.6 90.9 %reduce-scatter.2.cloned.1.call-start = ((), (), s32[]{:S(2)}) async-start(), calls=%async_computation.7 | async-start | bytes 1769472 | tf_op jit(solution)/shard_map/reduce_scatter | solution.py:80
  50.9 4.2 %copy-start.1 = (bf16[1,2048,704]{1,2,0:T(8,128)(2,1)S(1)}, bf16[1,2048,704]{1,2,0:T(8,128)(2,1)}, u32[]{:S(2)}) copy-start(bf16[1,2048,704]{1,2,0:T(8,128)(2,1)} %param.12) | copy-start | bytes 8650756
  50.9 4.2 %copy-start.7 = (bf16[4,96,2048]{2,1,0:T(8,128)(2,1)S(1)}, bf16[4,96,2048]{2,1,0:T(8,128)(2,1)}, u32[]{:S(2)}) copy-start(bf16[4,96,2048]{2,1,0:T(8,128)(2,1)} %all-gather.5.cloned.1.call-done) | copy-start | bytes 4718596
  84.3 1.4 copy-start.3
  84.3 2.0 %copy-start.2 = (bf16[1,2048,704]{1,2,0:T(8,128)(2,1)S(1)}, bf16[1,2048,704]{1,2,0:T(8,128)(2,1)}, u32[]{:S(2)}) copy-start(bf16[1,2048,704]{1,2,0:T(8,128)(2,1)} %param.12) | copy-start | bytes 8650756
  103.8 12.9 %all-to-all-start.3 = ((bf16[4,1,96]{2,1,0:T(2,128)(2,1)}), bf16[4,1,96]{2,1,0:T(2,128)(2,1)S(1)}, u32[]{:S(2)}, u32[]{:S(2)}) async-start(bf16[4,1,96]{2,1,0:T(2,128)(2,1)} %convert_element_type.83), calls=%async_computation.4 | async-start | bytes 4096 | tf_op jit(solution)/shard_map/all_to_all | solution.py:87
  108.4 5.0 %copy-start.4 = (bf16[384,704]{0,1:T(8,128)(2,1)S(1)}, bf16[384,704]{0,1:T(8,128)(2,1)}, u32[]{:S(2)}) copy-start(bf16[384,704]{0,1:T(8,128)(2,1)} %copy-done.3) | copy-start | bytes 1622020
  108.4 5.0 %copy-start.8 = (bf16[4,96,2048]{2,1,0:T(8,128)(2,1)S(1)}, bf16[4,96,2048]{2,1,0:T(8,128)(2,1)}, u32[]{:S(2)}) copy-start(bf16[4,96,2048]{2,1,0:T(8,128)(2,1)} %all-gather.5.cloned.1.call-done) | copy-start | bytes 4718596
  127.5 12.3 %all-to-all-start.2 = ((bf16[4,96,256]{2,1,0:T(8,128)(2,1)}), bf16[4,96,256]{2,1,0:T(8,128)(2,1)S(1)}, u32[]{:S(2)}, u32[]{:S(2)}) async-start(bf16[4,96,256]{2,1,0:T(8,128)(2,1)} %reduce-scatter.2.cloned.1.call-done), calls=%async_computation.3 | async-start | bytes 393216 | tf_op jit(solution)/shard_map/all_to_all | solution.py:84
Sparse Core Ops, SparseCore 0:
  26.0 24.8 all-gather.4
  52.8 25.7 all-gather.2
  89.1 38.3 reduce-scatter.1
where the time goes:
time: 149 us; the launch traced here: 148 us
  waiting for transfers between devices  45.9 us (31%)
  blocking collectives  36.7 us (25%)
  matrix products  31.3 us (21%)
  between operations  13.9 us (9%)
  starting transfers between devices  9.33 us (6%)
  local copies, waits for them, and re-layouts  8.1 us (5%)
  other arithmetic  3.1 us (2%)
    all_gather x1, waiting for transfers between devices, on_device(): lax.all_gather(recv_cotan, 'tp', axis=2, tiled=True)  20.8 us
    all_gather x1, waiting for transfers between devices, on_device(): lax.all_gather(recv_rows, 'tp', axis=2, tiled=True)  14.2 us
    all_to_all x1, blocking collectives, on_device(): lax.all_to_all(sent_rows.reshape(ep_size, capacity, slice_width), 'ep', s...  13.7 us
    psum x1, blocking collectives, on_device(): summed = lax.psum(slot_dots, 'tp')  13.1 us
    reduce_scatter x1, waiting for transfers between devices, on_device(): lax.psum_scatter(partial_value.reshape(ep_size, capacity, model_width), '...  10.8 us
    all_to_all x1, blocking collectives, on_device(): lax.all_to_all(sent_cotan.reshape(ep_size, capacity, slice_width), 'ep',...  9.87 us
    dot_general x1, matrix products, expert_grads(): hid_grad = jnp.dot(cotan, w_down.T, preferred_element_type=jnp.float32)  5.73 us
    dot_general x1, matrix products, expert_grads(): jnp.dot(rows.T, gate_part, preferred_element_type=jnp.float32)  5.03 us
  transfers between devices with their start and end apart: 5, of which 3 were waited for; matrix products, arithmetic and copies ran while one was open for 17% of the time, Pallas kernels for 0%

commit v1 on v0

--- a/solution.py
+++ b/solution.py
@@ -2,6 +2,15 @@
 import jax.numpy as jnp
 from jax import lax
 from jax.sharding import PartitionSpec as P
+
+
+def roots_time(vector):
+    vals = []
+    for _ in range(lax.axis_size("tp")):
+        vals.append(vector)
+    return jnp.concatenate(
+        lax.all_to_all(jnp.stack(vals), concat_axis=0, split_axis=0, axis_name="tp"), 2
+    )
 
 
 def expert_grads(rows, cotan, w_gate, w_up, w_down):
@@ -60,7 +69,7 @@
     )
     whole_rows, whole_cotan = (
         lax.all_gather(recv_rows, "tp", axis=2, tiled=True),
-        lax.all_gather(recv_cotan, "tp", axis=2, tiled=True),
+        roots_time(recv_cotan),
     )
     model_width = whole_rows.shape[2]
     rows = whole_rows.reshape(buffer_rows, model_width)

time: 149 us -> 138 us (0.926)
  waiting for transfers between devices: 45.9 us -> 9.52 us
  blocking collectives: 36.7 us -> 64.3 us
  matrix products: 31.3 us -> 26.8 us
  local copies, waits for them, and re-layouts: 8.1 us -> 10.6 us
    all_to_all x0 -> x1, blocking collectives: none -> 28.7 us  [roots_time(): lax.all_to_all(jnp.stack(vals), concat_axis=0, split_axis=0, axis_name='tp')]
    all_gather x1 -> x0, waiting for transfers between devices: 20.8 us -> none  [on_device(): lax.all_gather(recv_cotan, 'tp', axis=2, tiled=True)]
    all_gather x1, waiting for transfers between devices: 14.2 us -> 0.01 us  [on_device(): lax.all_gather(recv_rows, 'tp', axis=2, tiled=True)]
    dot_general x1, matrix products: 5.73 us -> 3.46 us  [expert_grads(): hid_grad = jnp.dot(cotan, w_down.T, preferred_element_type=jnp.float32)]
    unnamed x21 -> x32, local copies, waits for them, and re-layouts: 2.29 us -> 3.99 us
  transfers between devices with their start and end apart: 5 -> 4, of which waited for: 3 -> 1; matrix products, arithmetic and copies ran while one was open for 17% -> 16% of each run, Pallas kernels for 0% -> 0%
where the time goes in v1:
time: 138 us; the launch traced here: 137 us
  blocking collectives  64.3 us (47%)
  matrix products  26.8 us (19%)
  between operations  14.3 us (10%)
  local copies, waits for them, and re-layouts  10.6 us (8%)
  waiting for transfers between devices  9.52 us (7%)
  starting transfers between devices  8 us (6%)
  other arithmetic  3.76 us (3%)
    all_to_all x1, blocking collectives, roots_time(): lax.all_to_all(jnp.stack(vals), concat_axis=0, split_axis=0, axis_name='tp')  28.7 us
    all_to_all x1, blocking collectives, on_device(): lax.all_to_all(sent_rows.reshape(ep_size, capacity, slice_width), 'ep', s...  13.7 us
    psum x1, blocking collectives, on_device(): summed = lax.psum(slot_dots, 'tp')  12 us
    all_to_all x1, blocking collectives, on_device(): lax.all_to_all(sent_cotan.reshape(ep_size, capacity, slice_width), 'ep',...  9.94 us
    reduce_scatter x1, waiting for transfers between devices, on_device(): lax.psum_scatter(partial_value.reshape(ep_size, capacity, model_width), '...  9.48 us
    dot_general x1, matrix products, expert_grads(): jnp.dot(hidden.T, cotan, preferred_element_type=jnp.float32)  4.83 us
    dot_general x1, matrix products, expert_grads(): jnp.dot(rows.T, gate_part, preferred_element_type=jnp.float32)  4.79 us
    all_to_all x1, starting transfers between devices, on_device(): lax.all_to_all(row_sums.astype(jnp.bfloat16), 'ep', split_axis=0, concat_...  4.6 us
  transfers between devices with their start and end apart: 4, of which 1 were waited for; matrix products, arithmetic and copies ran while one was open for 16% of the time, Pallas kernels for 0%

profile of v1, /device:TPU:0, one launch (start us, length us, event | category | flops | bytes accessed | tf_op | source)
XLA Modules:
  0.0 137.3 jit_solution(1361706689343082679)
XLA Ops:
  7.2 0.9 copy.33
  8.5 1.2 reduce-window.6
  10.4 1.0 convolution_convert_fusion.3
  11.5 13.7 %all_to_all.26 = bf16[4,96,256]{2,1,0:T(8,128)(2,1)} all-to-all(bf16[4,96,256]{2,1,0:T(8,128)(2,1)S(1)} %bitcast.77), channel_id=1, replica_groups=mesh['ep'=4,'tp'=8] {'ep'}, dimensions={0} | all-to-all | bytes 393216 | tf_op jit(solution)/shard_map/all_to_all | solution.py:55
  26.1 9.9 %all_to_all.27 = bf16[4,96,256]{2,1,0:T(8,128)(2,1)S(1)} all-to-all(bf16[4,96,256]{2,1,0:T(8,128)(2,1)S(1)} %bitcast.76), channel_id=1, replica_groups=mesh['ep'=4,'tp'=8] {'ep'}, dimensions={0} | all-to-all | bytes 393216 | tf_op jit(solution)/shard_map/all_to_all | solution.py:62
  36.2 28.7 %all_to_all.28 = bf16[8,4,96,256]{3,2,1,0:T(8,128)(2,1)S(1)} all-to-all(bf16[8,4,96,256]{3,2,1,0:T(8,128)(2,1)S(1)} %stack.2), channel_id=1, replica_groups=mesh['ep'=4,'tp'=8] {'tp'}, dimensions={0} | all-to-all | bytes 3145728 | tf_op jit(solution)/shard_map/all_to_all | solution.py:12
  64.9 0.9 copy.40
  65.8 1.7 %copy.45 = bf16[48,8,8,256]{3,1,2,0:T(8,128)(2,1)} copy(bf16[48,8,8,256]{3,2,1,0:T(8,128)(2,1)S(1)} %bitcast.72) | data formatting | bytes 3145728
  67.4 3.2 %fusion.5 = f32[384,704]{0,1:T(8,128)S(1)} fusion(bf16[384,2048]{1,0:T(8,128)(2,1)} %bitcast.81, bf16[1,2048,704]{1,2,0:T(8,128)(2,1)S(1)} %copy-done), kind=kOutput, calls=%fused_computation.11 | convolution fusion | flops 1107296256 | bytes 5537792 | tf_op jit(solution)/shard_map/dot_general | solution.py:17
  70.7 1.7 %fusion.9 = f32[384,704]{0,1:T(8,128)S(1)} fusion(bf16[384,2048]{1,0:T(8,128)(2,1)S(1)} %bitcast.83, bf16[1,2048,704]{1,2,0:T(8,128)(2,1)S(1)} %copy-done.1), kind=kOutput, calls=%fused_computation.15 | convolution fusion | flops 1107296256 | bytes 5537792 | tf_op jit(solution)/shard_map/dot_general | solution.py:18
  73.0 3.5 %multiply_reduce_fusion = (f32[384]{0:T(512)}, bf16[384,704]{0,1:T(8,128)(2,1)}, bf16[384,704]{0,1:T(8,128)(2,1)S(1)}, bf16[384,704]{0,1:T(8,128)(2,1)S(1)}) fusion(f32[384,704]{0,1:T(8,128)S(1)} %fusion.9, f32[384,704]{0,1:T(8,128)S(1)} %fusion.5, bf16[384,2048]{1,0:T(8,128)(2,1)S(1)} %bitcast.75, bf16[1,704,2048]{2,1,0:T(8,128)(2,1)S(1)} %copy-done.11), kind=kOutput, calls=%fused_computation.23 | convolution fusion | flops 1112161920 | bytes 8242688 | tf_op jit(solution)/shard_map/dot_general | solution.py:21
  76.4 1.4 %fusion.3 = f32[384,2048]{1,0:T(8,128)S(1)} fusion(bf16[384,704]{0,1:T(8,128)(2,1)S(1)} %get-tuple-element.22, bf16[1,2048,704]{1,2,0:T(8,128)(2,1)S(1)} %copy-done), kind=kOutput, calls=%fused_computation.9 | convolution fusion | flops 1107296256 | bytes 6569984 | tf_op jit(solution)/shard_map/dot_general | solution.py:82
  77.9 2.7 %add_convert_fusion = bf16[384,2048]{1,0:T(8,128)(2,1)} fusion(f32[384,2048]{1,0:T(8,128)S(1)} %fusion.3, bf16[384,704]{0,1:T(8,128)(2,1)S(1)} %get-tuple-element.23, bf16[1,2048,704]{1,2,0:T(8,128)(2,1)S(1)} %copy-done.1), kind=kOutput, calls=%fused_computation.5 | convolution fusion | flops 1108869120 | bytes 8142848 | tf_op jit(solution)/shard_map/dot_general | solution.py:84
  80.6 0.7 mul.77
  82.6 12.0 %psum.7 = bf16[384]{0:T(512)(128)(2,1)S(1)} all-reduce(f32[384]{0:T(512)} %get-tuple-element.20), channel_id=1, replica_groups=mesh['ep'=4,'tp'=8] {'tp'}, use_global_device_ids=true, to_apply=%region_7.8 | all-reduce | flops 384 | bytes 2304 | tf_op jit(solution)/shard_map/psum | solution.py:88
  95.2 3.3 %all-to-all-start.4 = ((bf16[4,1,96]{2,1,0:T(2,128)(2,1)}), bf16[4,1,96]{2,1,0:T(2,128)(2,1)S(1)}, u32[]{:S(2)}, u32[]{:S(2)}) async-start(bf16[4,1,96]{2,1,0:T(2,128)(2,1)} %convert_element_type.83), calls=%async_computation.5 | async-start | bytes 4096 | tf_op jit(solution)/shard_map/all_to_all | solution.py:96
  98.5 4.8 %fusion.1 = bf16[1,2048,704]{1,2,0:T(8,128)(2,1)} fusion(bf16[384,704]{0,1:T(8,128)(2,1)S(1)} %get-tuple-element.22, bf16[384,2048]{1,0:T(8,128)(2,1)} %bitcast.82), kind=kOutput, calls=%fused_computation.7 | convolution fusion | flops 1108738048 | bytes 4997120 | tf_op jit(solution)/shard_map/dot_general | solution.py:29
  103.3 3.2 %fusion.2 = bf16[1,2048,704]{1,2,0:T(8,128)(2,1)} fusion(bf16[384,704]{0,1:T(8,128)(2,1)S(1)} %copy-done.4, bf16[384,2048]{1,0:T(8,128)(2,1)S(1)} %bitcast.84), kind=kOutput, calls=%fused_computation.8 | convolution fusion | flops 1108738048 | bytes 4997120 | tf_op jit(solution)/shard_map/dot_general | solution.py:30
  106.6 9.5 %reduce-scatter.2.cloned.1.call-done = bf16[4,96,256]{2,1,0:T(8,128)(2,1)} async-done(((bf16[4,96,2048]{2,1,0:T(8,128)(2,1)}), bf16[4,96,256]{2,1,0:T(8,128)(2,1)}) %reduce-scatter.2.cloned.1.call-update) | async-done | bytes 196624 | tf_op jit(solution)/shard_map/reduce_scatter | solution.py:89
  116.1 4.6 %all-to-all-start.3 = ((bf16[4,96,256]{2,1,0:T(8,128)(2,1)}), bf16[4,96,256]{2,1,0:T(8,128)(2,1)S(1)}, u32[]{:S(2)}, u32[]{:S(2)}) async-start(bf16[4,96,256]{2,1,0:T(8,128)(2,1)} %reduce-scatter.2.cloned.1.call-done), calls=%async_computation.4 | async-start | bytes 393216 | tf_op jit(solution)/shard_map/all_to_all | solution.py:93
  120.7 4.8 %fusion = bf16[1,704,2048]{2,1,0:T(8,128)(2,1)} fusion(bf16[384,704]{0,1:T(8,128)(2,1)} %get-tuple-element.21, bf16[384,2048]{1,0:T(8,128)(2,1)} %bitcast.74), kind=kOutput, calls=%fused_computation.6 | convolution fusion | flops 1108738048 | bytes 4997120 | tf_op jit(solution)/shard_map/dot_general | solution.py:28
  125.6 1.9 %gather_fusion.1 = f32[256]{0:T(256)S(1)} fusion(f32[384]{0:T(512)S(1)} %reshape.141, s32[1024]{0:T(1024)S(1)} %copy-done.7), kind=kCustom, calls=%fused_computation.1 | custom fusion | bytes 3072 | tf_op jit(solution)/shard_map/gather | solution.py:108
  128.4 1.0 gather_fusion
  129.5 0.9 reduce_sum.34
  (65 shorter events, 5.7 us)
Async XLA Ops:
  7.2 60.3 %copy-start = (bf16[1,2048,704]{1,2,0:T(8,128)(2,1)S(1)}, bf16[1,2048,704]{1,2,0:T(8,128)(2,1)}, u32[]{:S(2)}) copy-start(bf16[1,2048,704]{1,2,0:T(8,128)(2,1)} %param.11) | copy-start | bytes 8650756
  7.2 18.1 %copy-start.10 = (f32[128,2]{0,1:T(2,128)S(1)}, f32[128,2]{0,1:T(2,128)}, u32[]{:S(2)}) copy-start(f32[128,2]{0,1:T(2,128)} %param.10) | copy-start | bytes 3076
  7.2 18.7 %copy-start.5 = (bf16[128,256]{1,0:T(8,128)(2,1)S(1)}, bf16[128,256]{1,0:T(8,128)(2,1)}, u32[]{:S(2)}) copy-start(bf16[128,256]{1,0:T(8,128)(2,1)} %param.8) | copy-start | bytes 196612
  7.2 60.2 %all-gather.2.cloned.1.call-start = ((), (), s32[]{:S(2)}) async-start(), calls=%async_computation.6 | async-start | bytes 1769472 | tf_op jit(solution)/shard_map/all_gather | solution.py:71
  10.1 26.1 %copy-start.6 = (s32[256]{0:T(256)}, s32[256]{0:T(256)S(1)}, u32[]{:S(2)}) copy-start(s32[256]{0:T(256)S(1)} %fusion.21) | copy-start | bytes 3076
  25.2 90.8 %reduce-scatter.2.cloned.1.call-start = ((), (), s32[]{:S(2)}) async-start(), calls=%async_computation.7 | async-start | bytes 1769472 | tf_op jit(solution)/shard_map/reduce_scatter | solution.py:89
  67.4 3.2 %copy-start.1 = (bf16[1,2048,704]{1,2,0:T(8,128)(2,1)S(1)}, bf16[1,2048,704]{1,2,0:T(8,128)(2,1)}, u32[]{:S(2)}) copy-start(bf16[1,2048,704]{1,2,0:T(8,128)(2,1)} %param.12) | copy-start | bytes 8650756
  67.4 3.2 %copy-start.12 = (bf16[4,96,2048]{2,1,0:T(8,128)(2,1)S(1)}, bf16[4,96,2048]{2,1,0:T(8,128)(2,1)}, u32[]{:S(2)}) copy-start(bf16[4,96,2048]{2,1,0:T(8,128)(2,1)} %all-gather.2.cloned.1.call-done) | copy-start | bytes 4718596
  70.7 1.7 %copy-start.2 = (bf16[48,8,8,256]{3,1,2,0:T(8,128)(2,1)S(1)}, bf16[48,8,8,256]{3,1,2,0:T(8,128)(2,1)}, u32[]{:S(2)}) copy-start(bf16[48,8,8,256]{3,1,2,0:T(8,128)(2,1)} %copy.45) | copy-start | bytes 4718596
  70.7 2.3 %copy-start.11 = (bf16[1,704,2048]{2,1,0:T(8,128)(2,1)S(1)}, bf16[1,704,2048]{2,1,0:T(8,128)(2,1)}, u32[]{:S(2)}) copy-start(bf16[1,704,2048]{2,1,0:T(8,128)(2,1)} %param.13) | copy-start | bytes 8650756
  76.4 1.4 %copy-start.3 = (bf16[384,704]{0,1:T(8,128)(2,1)}, bf16[384,704]{0,1:T(8,128)(2,1)S(1)}, u32[]{:S(2)}) copy-start(bf16[384,704]{0,1:T(8,128)(2,1)S(1)} %get-tuple-element.23) | copy-start | bytes 1622020
  95.2 11.4 %all-to-all-start.4 = ((bf16[4,1,96]{2,1,0:T(2,128)(2,1)}), bf16[4,1,96]{2,1,0:T(2,128)(2,1)S(1)}, u32[]{:S(2)}, u32[]{:S(2)}) async-start(bf16[4,1,96]{2,1,0:T(2,128)(2,1)} %convert_element_type.83), calls=%async_computation.5 | async-start | bytes 4096 | tf_op jit(solution)/shard_map/all_to_all | solution.py:96
  98.5 4.8 %copy-start.4 = (bf16[384,704]{0,1:T(8,128)(2,1)S(1)}, bf16[384,704]{0,1:T(8,128)(2,1)}, u32[]{:S(2)}) copy-start(bf16[384,704]{0,1:T(8,128)(2,1)} %copy-done.3) | copy-start | bytes 1622020
  98.5 4.8 %copy-start.13 = (bf16[4,96,2048]{2,1,0:T(8,128)(2,1)S(1)}, bf16[4,96,2048]{2,1,0:T(8,128)(2,1)}, u32[]{:S(2)}) copy-start(bf16[4,96,2048]{2,1,0:T(8,128)(2,1)} %all-gather.2.cloned.1.call-done) | copy-start | bytes 4718596
  106.6 9.5 %copy-start.8 = (bf16[4,1,96]{2,1,0:T(2,128)(2,1)}, bf16[4,1,96]{2,1,0:T(2,128)(2,1)S(1)}, u32[]{:S(2)}) copy-start(bf16[4,1,96]{2,1,0:T(2,128)(2,1)S(1)} %all-to-all-done.4) | copy-start | bytes 2308
  116.1 12.3 %all-to-all-start.3 = ((bf16[4,96,256]{2,1,0:T(8,128)(2,1)}), bf16[4,96,256]{2,1,0:T(8,128)(2,1)S(1)}, u32[]{:S(2)}, u32[]{:S(2)}) async-start(bf16[4,96,256]{2,1,0:T(8,128)(2,1)} %reduce-scatter.2.cloned.1.call-done), calls=%async_computation.4 | async-start | bytes 393216 | tf_op jit(solution)/shard_map/all_to_all | solution.py:93
  120.7 4.8 %copy-start.9 = (bf16[4,1,96]{2,1,0:T(2,128)(2,1)S(1)}, bf16[4,1,96]{2,1,0:T(2,128)(2,1)}, u32[]{:S(2)}) copy-start(bf16[4,1,96]{2,1,0:T(2,128)(2,1)} %copy-done.8) | copy-start | bytes 2308
  120.7 4.9 %copy-start.7 = (s32[1024]{0:T(1024)S(1)}, s32[1024]{0:T(1024)}, u32[]{:S(2)}) copy-start(s32[1024]{0:T(1024)} %pad_clamp_fusion) | copy-start | bytes 12292
Sparse Core Ops, SparseCore 0:
  25.3 33.0 all-gather.1
  80.7 35.3 reduce-scatter.1
